TPU v7x, 128 devices: a whole 4x4x4 slice. The times are simulated.
128 devices in a mesh: sp: 16 (over z, y), tp: 8 (over x, core).
Axes of the slice: x: 4, y: 4, z: 4, core: 2. Of those that a mesh axis runs over, the one named last changes fastest.
Arguments:
- hidden_activations: bfloat16 [12288, 4096], P(('sp', 'tp')), may hold values from -6 to 6
- entry_rescale_vector: bfloat16 [4096], replicated, may hold values from 0.099609375 to 1.8984375
- probe_matrix: bfloat16 [4096, 2048], P('sp', 'tp'), may hold values from -0.09375 to 0.09375
- lookup_address_matrix: bfloat16 [4096, 2048], P('sp', 'tp'), may hold values from -0.09375 to 0.09375
- payload_matrix: bfloat16 [4096, 4096], P('sp', 'tp'), may hold values from -0.09375 to 0.09375
- postfilter_switch_matrix: bfloat16 [4096, 4096], P('sp', 'tp'), may hold values from -0.09375 to 0.09375
- prefilter_switch_matrix: bfloat16 [4096, 4096], P('sp', 'tp'), may hold values from -0.09375 to 0.09375
- filter_source_matrix: bfloat16 [4096, 4096], P('sp', 'tp'), may hold values from -0.09375 to 0.09375
- forget_left_factor: bfloat16 [4096, 64], replicated, may hold values from -0.09375 to 0.09375
- forget_right_factor: bfloat16 [64, 2048], P(None, 'tp'), may hold values from -0.75 to 0.75
- forget_offset_per_feature: float32 [2048], P('tp'), may hold values from -1 to 12
- forget_spike_additions: float32 [16, 12288], P('tp', 'sp'), may hold values from -3 to 0
- subspace_rescale_vector: bfloat16 [16, 256], P('tp'), may hold values from 0.099609375 to 1.8984375
- depthwise_filter_taps: bfloat16 [3, 4096], P(None, 'tp'), may hold values from -3.5 to 3.5
- mixer_result_matrix: bfloat16 [4096, 4096], P('tp'), may hold values from -0.09375 to 0.09375
- filter_result_matrix: bfloat16 [4096, 4096], P('tp'), may hold values from -0.09375 to 0.09375
Outputs:
- mixed: bfloat16 [12288, 4096], P(('sp', 'tp'))
All inputs are finite; a program needn't handle non-finite values.
Results may differ from a plain program's by a relative error of at most 0.02.
Values may be sent and summed in bfloat16 or wider, within the bound.
No kernel may reach another device: no remote copies, remote signals or barrier semaphores. Data moves between devices by JAX's collectives and lax.ppermute only.
A program may use at most 128 MiB of HBM per device.

v0:
```python
import jax
import jax.numpy as jnp
from jax import lax
from jax.sharding import Mesh
from jax.sharding import PartitionSpec as P

BLOCK = 64
SP = ("sp_0", "sp_1")
SP_TP = ("sp_0", "sp_1", "tp")
epsilon = 1e-06
softness_scale = 16.0


def nothing_yet(shard, identity):
    return jax.tree.map(
        lambda part, zero: jnp.zeros_like(part) + jnp.asarray(zero, part.dtype), shard, identity
    )


def entering(shard, axes, combine, identity):
    before = start = nothing_yet(shard, identity)
    total = shard
    for axis in reversed(axes):
        size, index = (lax.axis_size(axis), lax.axis_index(axis))
        pieces = jax.tree.map(
            lambda part, kind: lax.all_gather(part.astype(kind), axis),
            total,
            (jnp.bfloat16, jnp.bfloat16),
        )
        inside, total = (start, start)
        for k in range(size):
            passed = k < index
            total = combine(
                total, jax.tree.map(lambda part, own: part[k].astype(own.dtype), pieces, shard)
            )
            inside = jax.tree.map(lambda new, old: jnp.where(passed, new, old), total, inside)
        before = combine(inside, before)
    return before


def shifted(value, axis, steps):
    count = lax.axis_size(axis)
    leading, last = (max(0, -steps), min(count, count - steps))
    return lax.ppermute(value, axis, [(source, source + steps) for source in range(leading, last)])


def in_one_piece(arrays, axis, dim, along):
    both = jnp.concatenate(arrays, axis=along)
    out, at, gathered = (lax.all_gather(both, axis, axis=dim, tiled=True), 0, [])
    for a in arrays:
        gathered.append(lax.slice_in_dim(out, at, at + a.shape[along], axis=along))
        at += a.shape[along]
    return tuple(gathered)


def norm_values(rows, gain):
    rows_f = rows.astype(jnp.float32)
    meansq = jnp.mean(rows_f * rows_f, axis=-1, keepdims=True)
    return rows_f * lax.rsqrt(meansq + epsilon) * gain.astype(jnp.float32)


def row_norm(gain, rows):
    return norm_values(rows, gain).astype(jnp.bfloat16)


def project_rows(normalized_input):

    def accumulate(totals, weight_rows, offset):
        return tuple(
            (
                jnp.dot(normalized_input, rows_now, preferred_element_type=jnp.float32)
                for rows_now in weight_rows
            )
        )

    return accumulate


def empty_slots(normalized_input, weight_list):
    return tuple(
        (
            jnp.zeros((normalized_input.shape[0], weight.shape[1]), jnp.float32)
            for weight in weight_list
        )
    )


def block_terms(query_rows, key_rows, value_rows, forget_log_rate):
    length_value, head_number, key_dim = query_rows.shape
    value_dim = value_rows.shape[2]
    block_count = length_value // BLOCK
    key_shape = (block_count, BLOCK, head_number, key_dim)
    query_f32 = query_rows.astype(jnp.float32).reshape(key_shape) * key_dim ** (-0.5)
    key_f32 = key_rows.astype(jnp.float32).reshape(key_shape)
    value_f32 = value_rows.astype(jnp.float32).reshape(block_count, BLOCK, head_number, value_dim)
    within = jnp.cumsum(forget_log_rate.reshape(key_shape), axis=1)
    block_end = within[:, -1]
    query_decayed = query_f32 * jnp.exp(within)
    key_inverse = key_f32 * jnp.exp(-within)
    key_tail = key_f32 * jnp.exp(block_end[:, None] - within)
    highest = lax.Precision.HIGHEST
    scores = jnp.einsum("nihd,njhd->nhij", query_decayed, key_inverse, precision=highest)
    causal = jnp.tril(jnp.ones((BLOCK, BLOCK), dtype=bool))
    scores = jnp.where(causal, scores, 0.0)
    inside = jnp.einsum("nhij,njhv->nihv", scores, value_f32, precision=highest)
    updates = jnp.einsum("njhd,njhv->nhdv", key_tail, value_f32, precision=highest)

    def advance(state, pair):
        decay_now, update_now = pair
        return (jnp.exp(decay_now)[..., None] * state + update_now, state)

    start_state = jnp.zeros((head_number, key_dim, value_dim), jnp.float32)
    final_state, state_in = lax.scan(advance, start_state, (block_end, updates))
    carried = jnp.einsum("nihd,nhdv->nihv", query_decayed, state_in, precision=highest)
    return (inside + carried, query_decayed, block_end, final_state)


def chain_combine(earlier, later):
    return (earlier[0] * later[0], later[0][..., None] * earlier[1] + later[1])


def attention_path(
    normalized_input,
    sum_values,
    forget_left_factor,
    forget_right_factor,
    forget_offset_per_feature,
    forget_spike_additions,
    subspace_rescale_vector,
):
    length_value = normalized_input.shape[0]
    head_number = subspace_rescale_vector.shape[0]
    value_dim = subspace_rescale_vector.shape[1]
    query_rows = sum_values[0].astype(jnp.bfloat16).reshape(length_value, head_number, -1)
    key_rows = sum_values[1].astype(jnp.bfloat16).reshape(length_value, head_number, -1)
    value_rows = sum_values[2].astype(jnp.bfloat16).reshape(length_value, head_number, value_dim)
    low_rank = jnp.dot(
        normalized_input, forget_left_factor, preferred_element_type=jnp.float32
    ).astype(jnp.bfloat16)
    gate_preactivation = (
        jnp.dot(low_rank, forget_right_factor, preferred_element_type=jnp.float32)
        + forget_offset_per_feature
    )
    forget_log_rate = (jax.nn.log_sigmoid(gate_preactivation) / softness_scale).reshape(
        length_value, head_number, -1
    )
    forget_log_rate = forget_log_rate + jnp.transpose(forget_spike_additions)[:, :, None]
    local_out, query_decayed, block_end, final_state = block_terms(
        query_rows, key_rows, value_rows, forget_log_rate
    )
    prefix = jnp.cumsum(block_end, axis=0) - block_end
    query_far = query_decayed * jnp.exp(prefix)[:, None]
    total_decay = jnp.exp(jnp.sum(block_end, axis=0))
    identity = (jnp.ones_like(total_decay), jnp.zeros_like(final_state))
    incoming = entering((total_decay, final_state), SP, chain_combine, identity)[1]
    attended = local_out + jnp.einsum(
        "nihd,hdv->nihv", query_far, incoming, precision=lax.Precision.HIGHEST
    )
    attended = attended.reshape(length_value, head_number, value_dim)
    return (
        norm_values(attended, subspace_rescale_vector)
        .astype(jnp.bfloat16)
        .reshape(length_value, head_number * value_dim)
    )


def conv_branch(sum_values, depthwise_filter_taps):
    outer = sum_values[0].astype(jnp.bfloat16)
    inner = sum_values[1].astype(jnp.bfloat16)
    conv_in = sum_values[2].astype(jnp.bfloat16)
    length_value = outer.shape[0]
    gated_in = (inner.astype(jnp.float32) * conv_in.astype(jnp.float32)).astype(jnp.bfloat16)
    reach = depthwise_filter_taps.shape[0] - 1
    rim_rows = shifted(gated_in[length_value - reach :], SP, 1)
    padded = jnp.concatenate([rim_rows, gated_in], axis=0)
    taps_f32 = depthwise_filter_taps.astype(jnp.float32)
    conv_sum = jnp.zeros(outer.shape, jnp.float32)
    for tap_index in range(depthwise_filter_taps.shape[0]):
        conv_sum = conv_sum + taps_f32[tap_index] * padded[
            tap_index : tap_index + length_value
        ].astype(jnp.float32)
    return (conv_sum * outer.astype(jnp.float32)).astype(jnp.bfloat16)


def body(
    hidden_activations,
    entry_rescale_vector,
    probe_matrix,
    lookup_address_matrix,
    payload_matrix,
    postfilter_switch_matrix,
    prefilter_switch_matrix,
    filter_source_matrix,
    forget_left_factor,
    forget_right_factor,
    forget_offset_per_feature,
    forget_spike_additions,
    subspace_rescale_vector,
    depthwise_filter_taps,
    mixer_result_matrix,
    filter_result_matrix,
):
    normalized_input = row_norm(
        entry_rescale_vector, lax.all_gather(hidden_activations, "tp", axis=0, tiled=True)
    )
    accumulate = project_rows(normalized_input)
    attn_sums = accumulate(
        empty_slots(normalized_input, (probe_matrix, lookup_address_matrix, payload_matrix)),
        in_one_piece((probe_matrix, lookup_address_matrix, payload_matrix), SP, 0, 1),
        jnp.int32(0),
    )
    mixed_attn = attention_path(
        normalized_input,
        attn_sums,
        forget_left_factor,
        forget_right_factor,
        forget_offset_per_feature,
        forget_spike_additions,
        subspace_rescale_vector,
    )
    conv_sums = accumulate(
        empty_slots(
            normalized_input,
            (postfilter_switch_matrix, prefilter_switch_matrix, filter_source_matrix),
        ),
        in_one_piece(
            (postfilter_switch_matrix, prefilter_switch_matrix, filter_source_matrix), SP, 0, 1
        ),
        jnp.int32(0),
    )
    mixed_conv = conv_branch(conv_sums, depthwise_filter_taps)
    return lax.psum_scatter(
        (
            jnp.dot(mixed_attn, mixer_result_matrix, preferred_element_type=jnp.float32)
            + jnp.dot(mixed_conv, filter_result_matrix, preferred_element_type=jnp.float32)
        ).astype(jnp.bfloat16),
        "tp",
        scatter_dimension=0,
        tiled=True,
    )


def solution(mesh):
    split = Mesh(mesh.devices.reshape(4, 4, mesh.shape["tp"]), ("sp_0", "sp_1", "tp"))
    in_specs = (
        P(SP_TP, None),
        P(),
        P(SP, "tp"),
        P(SP, "tp"),
        P(SP, "tp"),
        P(SP, "tp"),
        P(SP, "tp"),
        P(SP, "tp"),
        P(),
        P(None, "tp"),
        P("tp"),
        P("tp", SP),
        P("tp", None),
        P(None, "tp"),
        P("tp", None),
        P("tp", None),
    )
    out_specs = P(SP_TP, None)
    return jax.shard_map(body, mesh=split, in_specs=in_specs, out_specs=out_specs, check_vma=False)
```

profile of v0, /device:TPU:1, one launch (start us, length us, event | category | flops | bytes accessed | tf_op | source)
XLA Modules:
  0.0 311.4 jit_solution(12454789588959216576)
XLA Ops:
  7.3 1.9 pad_maximum_fusion.3
  9.3 2.1 pad_maximum_fusion.2
  11.8 41.7 %all-gather.7.cloned.1.call-done = bf16[768,4096]{1,0:T(8,128)(2,1)} async-done(((bf16[96,4096]{1,0:T(8,128)(2,1)}), bf16[768,4096]{1,0:T(8,128)(2,1)}) %all-gather.7.cloned.1.call-update) | async-done | bytes 6291472 | tf_op jit(solution)/shard_map/all_gather | solution.py:204
  53.5 4.2 %fusion = f32[768]{0:T(1024)S(1)} fusion(bf16[768,4096]{1,0:T(8,128)(2,1)} %all-gather.7.cloned.1.call-done), kind=kLoop, calls=%fused_computation.6 | loop fusion | flops 9436416 | bytes 6294528 | tf_op jit(solution)/shard_map/reduce_sum | solution.py:58
  58.1 5.4 %fusion.2 = bf16[768,4096]{1,0:T(8,128)(2,1)} fusion(bf16[768,4096]{1,0:T(8,128)(2,1)S(1)} %copy-done.2, f32[4096]{0:T(1024)S(1)} %convert_element_type.265, f32[768]{0:T(1024)S(1)} %add_rsqrt_fusion.1), kind=kLoop, calls=%fused_computation.8 | loop fusion | flops 12582912 | bytes 12602368 | tf_op jit(solution)/shard_map/convert_element_type | solution.py:63
  63.5 5.7 %fusion.49 = f32[768,256]{1,0:T(8,128)S(1)} fusion(bf16[64,256]{1,0:T(8,128)(2,1)S(1)} %copy-done.13, bf16[768,4096]{1,0:T(8,128)(2,1)} %fusion.2, bf16[4096,64]{0,1:T(8,128)(2,1)S(1)} %copy-done, f32[256]{0:T(256)S(1)} %copy-done.14), kind=kOutput, calls=%fused_computation.51 | convolution fusion | flops 429834240 | bytes 7635968 | tf_op jit(solution)/shard_map/dot_general | solution.py:141
  70.5 8.2 %all-gather.2 = bf16[4,2,128]{2,1,0:T(2,128)(2,1)S(1)} all-gather(bf16[1,2,128]{2,1,0:T(2,128)(2,1)S(1)} %fusion.121), channel_id=2, replica_groups=mesh['sp_0'=4,'sp_1'=4,'tp'=8] {'sp_1'}, dimensions={0}, use_global_device_ids=true | all-gather | bytes 2560 | tf_op jit(solution)/shard_map/all_gather | solution.py:26
  78.7 8.3 %all_gather.30 = bf16[4,2,128]{2,1,0:T(2,128)(2,1)S(1)} all-gather(bf16[1,2,128]{2,1,0:T(2,128)(2,1)S(1)} %get-tuple-element.96), channel_id=1, replica_groups=mesh['sp_0'=4,'sp_1'=4,'tp'=8] {'sp_0'}, dimensions={0}, use_global_device_ids=true | all-gather | bytes 2560 | tf_op jit(solution)/shard_map/all_gather | solution.py:26
  87.0 39.1 %all-gather.9.cloned.1.call-done = bf16[4096,1024]{1,0:T(8,128)(2,1)} async-done(((bf16[256,1024]{1,0:T(8,128)(2,1)}), bf16[4096,1024]{1,0:T(8,128)(2,1)}) %all-gather.9.cloned.1.call-update) | async-done | bytes 8388624 | tf_op jit(solution)/shard_map/all_gather | solution.py:49
  126.1 5.2 %fusion.42 = f32[768,256]{1,0:T(8,128)S(1)} fusion(bf16[768,4096]{1,0:T(8,128)(2,1)} %fusion.2, bf16[4096,1024]{1,0:T(8,128)(2,1)} %all-gather.9.cloned.1.call-done), kind=kOutput, calls=%fused_computation.39 | convolution fusion | flops 1611005952 | bytes 9175040 | tf_op jit(solution)/shard_map/dot_general | solution.py:71
  131.7 7.4 %fusion.15 = bf16[768,512]{1,0:T(8,128)(2,1)S(1)} fusion(bf16[768,4096]{1,0:T(8,128)(2,1)} %fusion.2, bf16[4096,1024]{1,0:T(8,128)(2,1)} %all-gather.9.cloned.1.call-done), kind=kOutput, calls=%fused_computation.28 | convolution fusion | flops 3221618688 | bytes 11272192 | tf_op jit(solution)/shard_map/dot_general | solution.py:71
  139.4 5.4 %fusion.36 = f32[768,256]{1,0:T(8,128)S(1)} fusion(bf16[768,4096]{1,0:T(8,128)(2,1)} %fusion.2, bf16[4096,1024]{1,0:T(8,128)(2,1)} %all-gather.9.cloned.1.call-done), kind=kOutput, calls=%fused_computation.37 | convolution fusion | flops 1611202560 | bytes 9175040 | tf_op jit(solution)/shard_map/dot_general | solution.py:71
  144.7 1.3 mul.250
  146.0 3.9 %copy_multiply_fusion = (f32[12,64,2,128]{3,0,1,2:T(8,128)S(1)}, f32[12,64,2,128]{3,0,1,2:T(8,128)}, f32[12,64,2,128]{3,0,1,2:T(8,128)}, f32[12,64,2,128]{3,0,1,2:T(8,128)S(1)}) fusion(f32[12,64,2,128]{3,2,1,0:T(2,128)S(1)} %reshape.177, f32[12,64,2,128]{3,0,1,2:T(8,128)} %copy-done.5, f32[12,2,128]{2,0,1:T(8,128)S(1)} %get-tuple-element.140, ...), kind=kLoop, calls=%fused_computation.41 | loop fusion | flops 1179648 | bytes 5529600 | tf_op jit(solution)/shard_map/mul | solution.py:100
  149.9 3.2 %fusion.52 = f32[12,2,128,256]{3,2,1,0:T(8,128)} fusion(f32[12,64,2,128]{3,0,1,2:T(8,128)S(1)} %get-tuple-element.85, bf16[12,64,2,256]{3,2,1,0:T(2,128)(2,1)S(1)} %reshape.174), kind=kOutput, calls=%fused_computation.56 | convolution fusion | flops 603979776 | bytes 4718592 | tf_op jit(solution)/shard_map/njhd,njhv->nhdv/dot_general | solution.py:106
  153.1 22.3 %while.13 = (s32[]{:T(128)}, f32[2,128,256]{2,1,0:T(8,128)S(1)}, f32[12,2,128,256]{3,2,1,0:T(8,128)}, f32[12,2,128]{2,0,1:T(8,128)S(1)}, f32[12,2,128,256]{3,2,1,0:T(8,128)}, /*index=5*/s32[]{:T(128)}, s32[]{:T(128)}) while((s32[]{:T(128)}, f32[2,128,256]{2,1,0:T(8,128)S(1)}, f32[12,2,128,256]{3,2,1,0:T(8,128)}, ...), condition=%wide.region_3.4_spmd.clone, body=%wide.region_2.3_spmd.clone.sunk | while | flops 262147 | bytes 1315948 | solution.py:113
  164.9 1.1 bitcast_add_fusion.3
  175.4 14.8 %all-gather.1 = bf16[8,128,256]{2,1,0:T(8,128)(2,1)S(1)} all-gather(bf16[2,128,256]{2,1,0:T(8,128)(2,1)S(1)} %convert_element_type.296), channel_id=3, replica_groups=mesh['sp_0'=4,'sp_1'=4,'tp'=8] {'sp_1'}, dimensions={0}, use_global_device_ids=true | all-gather | bytes 655360 | tf_op jit(solution)/shard_map/all_gather | solution.py:26
  190.4 14.6 %all_gather.33 = bf16[4,2,128,256]{3,2,1,0:T(8,128)(2,1)S(1)} all-gather(bf16[1,2,128,256]{3,2,1,0:T(8,128)(2,1)S(1)} %fusion.81), channel_id=1, replica_groups=mesh['sp_0'=4,'sp_1'=4,'tp'=8] {'sp_0'}, dimensions={0}, use_global_device_ids=true | all-gather | bytes 655360 | tf_op jit(solution)/shard_map/all_gather | solution.py:26
  205.0 3.1 convolution_select_fusion
  208.9 2.1 fusion.62
  211.0 3.4 %multiply_reduce_fusion = (f32[12,64,2]{1,2,0:T(2,128)S(1)}, f32[12,64,2,256]{3,1,2,0:T(8,128)}) fusion(f32[12,64,2,128]{3,0,1,2:T(8,128)S(1)} %copy-done.7, bf16[4,2,128,256]{3,2,1,0:T(8,128)(2,1)S(1)} %all_gather.33, f32[2,128]{1,0:T(2,128)S(1)} %get-tuple-element.97, f32[2,128]{1,0:T(2,128)S(1)} %get-tuple-element.103, ...), kind=kOutput, calls=%fused_computation.27 | convolution fusion | flops 607648256 | bytes 6568968 | tf_op jit(solution)/shard_map/nihd,hdv->nihv/dot_general | solution.py:156
  214.6 1.2 mul.290
  216.0 1.2 copy.69
  217.2 1.3 copy.75
  218.5 3.5 %all-gather.11.cloned.1.call-done = bf16[4096,1536]{1,0:T(8,128)(2,1)} async-done(((bf16[256,1536]{1,0:T(8,128)(2,1)}), bf16[4096,1536]{1,0:T(8,128)(2,1)}) %all-gather.11.cloned.1.call-update) | async-done | bytes 12582928 | tf_op jit(solution)/shard_map/all_gather | solution.py:49
  222.0 7.4 %fusion.18 = bf16[768,512]{1,0:T(8,128)(2,1)S(1)} fusion(bf16[768,4096]{1,0:T(8,128)(2,1)} %fusion.2, bf16[4096,1536]{1,0:T(8,128)(2,1)} %all-gather.11.cloned.1.call-done), kind=kOutput, calls=%fused_computation.29 | convolution fusion | flops 3221618688 | bytes 11272192 | tf_op jit(solution)/shard_map/dot_general | solution.py:71
  229.4 7.6 %multiply_convert_fusion.1 = bf16[768,512]{1,0:T(8,128)(2,1)S(1)} fusion(bf16[768,512]{1,0:T(8,128)(2,1)S(1)} %fusion.18, bf16[768,4096]{1,0:T(8,128)(2,1)} %fusion.2, bf16[4096,1536]{1,0:T(8,128)(2,1)} %all-gather.11.cloned.1.call-done), kind=kOutput, calls=%fused_computation.25 | convolution fusion | flops 3223191552 | bytes 12058624 | tf_op jit(solution)/shard_map/dot_general | solution.py:71
  237.0 3.1 collective-permute-start
  240.2 6.4 %fusion.47 = f32[768,4096]{1,0:T(8,128)} fusion(bf16[512,4096]{1,0:T(8,128)(2,1)S(1)} %copy-done.6, f32[768,512]{1,0:T(8,128)S(1)} %bitcast.180, f32[768,512]{1,0:T(8,128)S(1)} %bitcast.179, f32[512]{0:T(512)S(1)} %bitcast.185), kind=kOutput, calls=%fused_computation.49 | convolution fusion | flops 3222405120 | bytes 19924992 | tf_op jit(solution)/shard_map/dot_general | solution.py:234
  246.6 15.3 %add_convert_fusion = bf16[768,4096]{1,0:T(8,128)(2,1)} fusion(f32[768,4096]{1,0:T(8,128)} %fusion.47, bf16[512,4096]{1,0:T(8,128)(2,1)} %param.33, bf16[768,512]{1,0:T(8,128)(2,1)S(1)} %multiply_convert_fusion.1, bf16[2,512]{1,0:T(2,128)(2,1)S(1)} %collective-permute-done, f32[512]{0:T(512)S(1)} %bitcast.189, f32[512]{0:T(512)S(1)} %bitcast.188, ...), kind=kOutput, calls=%fused_computation.9 | convolution fusion | flops 6455820288 | bytes 34349056 | tf_op jit(solution)/shard_map/dot_general | solution.py:235
  261.9 43.0 %reduce-scatter.2.cloned.1.call-done = bf16[96,4096]{1,0:T(8,128)(2,1)} async-done(((bf16[768,4096]{1,0:T(8,128)(2,1)}), bf16[96,4096]{1,0:T(8,128)(2,1)}) %reduce-scatter.2.cloned.1.call-update) | async-done | bytes 786448 | tf_op jit(solution)/shard_map/reduce_scatter | solution.py:232
  (115 shorter events, 25.4 us)
Async XLA Ops:
  6.5 57.0 %copy-start = (bf16[4096,64]{0,1:T(8,128)(2,1)S(1)}, bf16[4096,64]{0,1:T(8,128)(2,1)}, u32[]{:S(2)}) copy-start(bf16[4096,64]{0,1:T(8,128)(2,1)} %param.26) | copy-start | bytes 1572868
  6.5 4.9 %copy-start.12 = (bf16[2,256]{1,0:T(2,128)(2,1)S(1)}, bf16[2,256]{1,0:T(2,128)(2,1)}, u32[]{:S(2)}) copy-start(bf16[2,256]{1,0:T(2,128)(2,1)} %param.30) | copy-start | bytes 3076
  6.5 5.0 %copy-start.10 = (bf16[4096]{0:T(1024)(128)(2,1)S(1)}, bf16[4096]{0:T(1024)(128)(2,1)}, u32[]{:S(2)}) copy-start(bf16[4096]{0:T(1024)(128)(2,1)} %param.19) | copy-start | bytes 24580
  6.5 5.0 %copy-start.11 = (f32[2,768]{1,0:T(2,128)S(1)}, f32[2,768]{1,0:T(2,128)}, u32[]{:S(2)}) copy-start(f32[2,768]{1,0:T(2,128)} %param.29) | copy-start | bytes 18436
  6.5 5.2 %copy-start.9 = (bf16[3,512]{1,0:T(4,128)(2,1)S(1)}, bf16[3,512]{1,0:T(4,128)(2,1)}, u32[]{:S(2)}) copy-start(bf16[3,512]{1,0:T(4,128)(2,1)} %param.31) | copy-start | bytes 9220
  6.5 46.9 %all-gather.7.cloned.1.call-start = ((), (), s32[]{:S(2)}) async-start(), calls=%async_computation.1 | async-start | bytes 7077888 | tf_op jit(solution)/shard_map/all_gather | solution.py:204
  7.3 118.8 %all-gather.9.cloned.1.call-start = ((), (), s32[]{:S(2)}) async-start(), calls=%async_computation.2 | async-start | bytes 8912896 | tf_op jit(solution)/shard_map/all_gather | solution.py:49
  9.2 212.8 %all-gather.11.cloned.1.call-start = ((), (), s32[]{:S(2)}) async-start(), calls=%async_computation.3 | async-start | bytes 13369344 | tf_op jit(solution)/shard_map/all_gather | solution.py:49
  11.4 293.5 %reduce-scatter.2.cloned.1.call-start = ((), (), s32[]{:S(2)}) async-start(), calls=%async_computation.4 | async-start | bytes 7077888 | tf_op jit(solution)/shard_map/reduce_scatter | solution.py:232
  53.5 4.6 %copy-start.2 = (bf16[768,4096]{1,0:T(8,128)(2,1)S(1)}, bf16[768,4096]{1,0:T(8,128)(2,1)}, u32[]{:S(2)}) copy-start(bf16[768,4096]{1,0:T(8,128)(2,1)} %all-gather.7.cloned.1.call-done) | copy-start | bytes 18874372
  58.1 5.4 %copy-start.13 = (bf16[64,256]{1,0:T(8,128)(2,1)S(1)}, bf16[64,256]{1,0:T(8,128)(2,1)}, u32[]{:S(2)}) copy-start(bf16[64,256]{1,0:T(8,128)(2,1)} %param.27) | copy-start | bytes 98308
  58.1 5.4 %copy-start.14 = (f32[256]{0:T(256)S(1)}, f32[256]{0:T(256)}, u32[]{:S(2)}) copy-start(f32[256]{0:T(256)} %param.28) | copy-start | bytes 3076
  70.4 60.9 %copy-start.5 = (f32[12,64,2,128]{3,0,1,2:T(8,128)}, f32[12,64,2,128]{3,0,1,2:T(8,128)S(1)}, u32[]{:S(2)}) copy-start(f32[12,64,2,128]{3,0,1,2:T(8,128)S(1)} %fusion.45) | copy-start | bytes 2359300
  175.3 33.6 %copy-start.8 = (f32[12,2,128,256]{3,2,1,0:T(8,128)S(1)}, f32[12,2,128,256]{3,2,1,0:T(8,128)}, u32[]{:S(2)}) copy-start(f32[12,2,128,256]{3,2,1,0:T(8,128)} %get-tuple-element.33) | copy-start | bytes 9437188
  208.1 2.9 copy-start.7
  214.6 1.4 copy-start.4
  229.4 10.7 %copy-start.3 = (f32[96,8,2,256]{3,1,2,0:T(8,128)S(1)}, f32[96,8,2,256]{3,1,2,0:T(8,128)}, u32[]{:S(2)}) copy-start(f32[96,8,2,256]{3,1,2,0:T(8,128)} %copy.75) | copy-start | bytes 4718596
  229.4 10.7 %copy-start.6 = (bf16[512,4096]{1,0:T(8,128)(2,1)S(1)}, bf16[512,4096]{1,0:T(8,128)(2,1)}, u32[]{:S(2)}) copy-start(bf16[512,4096]{1,0:T(8,128)(2,1)} %param.32) | copy-start | bytes 12582916
  237.0 9.5 %collective-permute-start = (bf16[2,512]{1,0:T(2,128)(2,1)S(1)}, bf16[2,512]{1,0:T(2,128)(2,1)S(1)}, u32[]{:S(2)}, u32[]{:S(2)}) collective-permute-start(bf16[2,512]{1,0:T(2,128)(2,1)S(1)} %slice.151), channel_id=1, source_target_pairs={{0,8},{8,16},{16,24},{24,32},{32,40},{40,48},{48,56},{56,64},{64,7... | collective-permute-start | bytes 6152 | tf_op jit(solution)/shard_map/ppermute | solution.py:44
  246.6 58.4 %copy-start.1 = (bf16[4096,64]{0,1:T(8,128)(2,1)S(1)}, bf16[4096,64]{0,1:T(8,128)(2,1)}, u32[]{:S(2)}) copy-start(bf16[4096,64]{0,1:T(8,128)(2,1)} %param.26) | copy-start | bytes 1572868
Sparse Core Ops, SparseCore 0:
  9.0 44.4 all-gather.6
  55.6 70.4 all-gather.8
  128.3 93.7 all-gather.10
  262.0 42.8 reduce-scatter.1
where the time goes:
time: 312 us; the launch traced here: 311 us
  waiting for transfers between devices  128 us (41%)
  matrix products  72.9 us (23%)
  blocking collectives  45.9 us (15%)
  other arithmetic  40.2 us (13%)
  between operations  13.5 us (4%)
  local copies, waits for them, and re-layouts  7.15 us (2%)
  starting transfers between devices  3.27 us (1%)
    all_gather x4, blocking collectives, entering(): lax.all_gather(part.astype(kind), axis)  45.9 us
    reduce_scatter x1, waiting for transfers between devices, body(): lax.psum_scatter((jnp.dot(mixed_attn, mixer_result_matrix, preferred_elem...  43 us
    all_gather x2, waiting for transfers between devices, in_one_piece(): lax.all_gather(both, axis, axis=dim, tiled=True)  42.6 us
    all_gather x1, waiting for transfers between devices, body(): lax.all_gather(hidden_activations, 'tp', axis=0, tiled=True)  41.7 us
    dot_general x5, matrix products, accumulate(): jnp.dot(normalized_input, rows_now, preferred_element_type=jnp.float32)  32.9 us
    dot_general x1, matrix products, body(): jnp.dot(mixed_conv, filter_result_matrix, preferred_element_type=jnp.floa...  15.3 us
    add x12, other arithmetic, advance(): return (jnp.exp(decay_now)[..., None] * state + update_now, state)  12.9 us
    dynamic_update_slice x12, other arithmetic, block_terms(): final_state, state_in = lax.scan(advance, start_state, (block_end, updates))  8.77 us
  transfers between devices with their start and end apart: 5, of which 4 were waited for; matrix products, arithmetic and copies ran while one was open for 29% of the time, Pallas kernels for 0%

commit v1 on v0

--- a/solution.py
+++ b/solution.py
@@ -9,6 +9,28 @@
 SP_TP = ("sp_0", "sp_1", "tp")
 epsilon = 1e-06
 softness_scale = 16.0
+
+
+def in_order(pieces, dim):
+    shape = list(pieces.shape[1:])
+    shape[dim] *= pieces.shape[0]
+    return jnp.moveaxis(pieces, 0, dim).reshape(shape)
+
+
+def gather_around(x, axis, dim):
+    size = lax.axis_size(axis)
+    pairs = [(i, (i + 1) % size) for i in range(size)]
+    back = [(b, a) for a, b in pairs]
+    lower, upper = ([], [])
+    for lap in range(size - 1):
+        if lap % 2 == 0:
+            lower.append(lax.ppermute(lower[-1] if lower else x, axis, pairs))
+        else:
+            upper.append(lax.ppermute(upper[-1] if upper else x, axis, back))
+    blocks = jnp.stack([*lower[::-1], x, *upper])
+    shift = lax.axis_index(axis) - len(lower)
+    blocks = blocks[(jnp.arange(size) - shift) % size]
+    return in_order(blocks, dim)
 
 
 def nothing_yet(shard, identity):
@@ -200,9 +222,7 @@
     mixer_result_matrix,
     filter_result_matrix,
 ):
-    normalized_input = row_norm(
-        entry_rescale_vector, lax.all_gather(hidden_activations, "tp", axis=0, tiled=True)
-    )
+    normalized_input = row_norm(entry_rescale_vector, gather_around(hidden_activations, "tp", 0))
     accumulate = project_rows(normalized_input)
     attn_sums = accumulate(
         empty_slots(normalized_input, (probe_matrix, lookup_address_matrix, payload_matrix)),

time: 312 us -> 296 us (0.949)
  waiting for transfers between devices: 128 us -> 79.4 us
  local copies, waits for them, and re-layouts: 7.15 us -> 27.1 us
  starting transfers between devices: 3.27 us -> 15.1 us
  other arithmetic: 40.2 us -> 44.4 us
    all_gather x2, waiting for transfers between devices: 42.6 us -> 0.02 us  [in_one_piece(): lax.all_gather(both, axis, axis=dim, tiled=True)]
    all_gather x1 -> x0, waiting for transfers between devices: 41.7 us -> none  [body(): lax.all_gather(hidden_activations, 'tp', axis=0, tiled=True)]
    ppermute x0 -> x7, waiting for transfers between devices: none -> 27.7 us  [the longest x4 27.7 us: gather_around(): lower.append(lax.ppermute(lower[-1] if lower else x, axis, pairs))]
    ppermute x0 -> x7, starting transfers between devices: none -> 13.7 us  [the longest x4 10 us: gather_around(): lower.append(lax.ppermute(lower[-1] if lower else x, axis, pairs))]
    unnamed x33 -> x32, local copies, waits for them, and re-layouts: 1.87 us -> 12.8 us
    reduce_scatter x1, waiting for transfers between devices: 43 us -> 51.6 us  [body(): lax.psum_scatter((jnp.dot(mixed_attn, mixer_result_matrix, preferred_elem...]
    gather x0 -> x1, local copies, waits for them, and re-layouts: none -> 6.53 us  [gather_around(): blocks = blocks[(jnp.arange(size) - shift) % size]]
  transfers between devices with their start and end apart: 5 -> 11, of which waited for: 4 -> 5; matrix products, arithmetic and copies ran while one was open for 29% -> 38% of each run, Pallas kernels for 0% -> 0%
where the time goes in v1:
time: 296 us; the launch traced here: 295 us
  waiting for transfers between devices  79.4 us (27%)
  matrix products  72.3 us (24%)
  other arithmetic  44.4 us (15%)
  blocking collectives  43 us (15%)
  local copies, waits for them, and re-layouts  27.1 us (9%)
  starting transfers between devices  15.1 us (5%)
  between operations  13.5 us (5%)
    reduce_scatter x1, waiting for transfers between devices, body(): lax.psum_scatter((jnp.dot(mixed_attn, mixer_result_matrix, preferred_elem...  51.6 us
    all_gather x4, blocking collectives, entering(): lax.all_gather(part.astype(kind), axis)  43 us
    dot_general x5, matrix products, accumulate(): jnp.dot(normalized_input, rows_now, preferred_element_type=jnp.float32)  32.8 us
    ppermute x4, waiting for transfers between devices, gather_around(): lower.append(lax.ppermute(lower[-1] if lower else x, axis, pairs))  27.7 us
    dot_general x1, matrix products, body(): jnp.dot(mixed_conv, filter_result_matrix, preferred_element_type=jnp.floa...  15.3 us
    add x12, other arithmetic, advance(): return (jnp.exp(decay_now)[..., None] * state + update_now, state)  12.9 us
    unnamed x32, local copies, waits for them, and re-layouts  12.8 us
    ppermute x4, starting transfers between devices, gather_around(): lower.append(lax.ppermute(lower[-1] if lower else x, axis, pairs))  10 us
  transfers between devices with their start and end apart: 11, of which 5 were waited for; matrix products, arithmetic and copies ran while one was open for 38% of the time, Pallas kernels for 0%

profile of v1, /device:TPU:1, one launch (start us, length us, event | category | flops | bytes accessed | tf_op | source)
XLA Modules:
  0.0 295.0 jit_solution(6194945593022002809)
XLA Ops:
  8.6 2.6 collective-permute-start
  11.2 9.3 %collective-permute-done = bf16[96,4096]{1,0:T(8,128)(2,1)S(1)} collective-permute-done((bf16[96,4096]{1,0:T(8,128)(2,1)}, bf16[96,4096]{1,0:T(8,128)(2,1)S(1)}, u32[]{:S(2)}, u32[]{:S(2)}) %collective-permute-start) | collective-permute-done | bytes 786464 | tf_op jit(solution)/shard_map/ppermute | solution.py:27
  20.4 2.4 collective-permute-start.1
  22.8 8.9 %collective-permute-done.1 = bf16[96,4096]{1,0:T(8,128)(2,1)} collective-permute-done((bf16[96,4096]{1,0:T(8,128)(2,1)S(1)}, bf16[96,4096]{1,0:T(8,128)(2,1)}, u32[]{:S(2)}, u32[]{:S(2)}) %collective-permute-start.1) | collective-permute-done | bytes 786464 | tf_op jit(solution)/shard_map/ppermute | solution.py:27
  31.7 2.6 collective-permute-start.2
  37.7 5.8 %collective-permute-done.2 = bf16[96,4096]{1,0:T(8,128)(2,1)} collective-permute-done((bf16[96,4096]{1,0:T(8,128)(2,1)}, bf16[96,4096]{1,0:T(8,128)(2,1)}, u32[]{:S(2)}, u32[]{:S(2)}) %collective-permute-start.2) | collective-permute-done | bytes 786464 | tf_op jit(solution)/shard_map/ppermute | solution.py:27
  43.6 2.5 collective-permute-start.3
  49.2 2.4 collective-permute-start.6
  51.6 3.7 %collective-permute-done.3 = bf16[96,4096]{1,0:T(8,128)(2,1)} collective-permute-done((bf16[96,4096]{1,0:T(8,128)(2,1)}, bf16[96,4096]{1,0:T(8,128)(2,1)}, u32[]{:S(2)}, u32[]{:S(2)}) %collective-permute-start.3) | collective-permute-done | bytes 786464 | tf_op jit(solution)/shard_map/ppermute | solution.py:27
  55.3 2.1 bitcast_dynamic-update-slice_fusion.8
  64.5 2.1 bitcast_dynamic-update-slice_fusion.2
  67.6 6.5 %gather_fusion = bf16[8,96,4096]{2,1,0:T(8,128)(2,1)} fusion(bf16[8,96,4096]{2,1,0:T(8,128)(2,1)} %bitcast_dynamic-update-slice_fusion.1, s32[1024]{0:T(1024)S(1)} %pad_clamp_fusion), kind=kCustom, calls=%fused_computation | custom fusion | bytes 12582944 | tf_op jit(solution)/shard_map/gather | solution.py:32
  74.1 4.1 %multiply_reduce_fusion = f32[8,96]{1,0:T(8,128)S(1)} fusion(bf16[8,96,4096]{2,1,0:T(8,128)(2,1)} %gather_fusion), kind=kLoop, calls=%fused_computation.9 | loop fusion | flops 9436416 | bytes 6294528 | tf_op jit(solution)/shard_map/reduce_sum | solution.py:80
  78.3 8.2 %fusion.1 = bf16[768,4096]{1,0:T(8,128)(2,1)} fusion(f32[4096]{0:T(1024)S(1)} %convert_element_type.273, f32[768]{0:T(1024)S(1)} %rsqrt.23, bf16[8,96,4096]{2,1,0:T(8,128)(2,1)} %gather_fusion), kind=kLoop, calls=%fused_computation.7 | loop fusion | flops 12582912 | bytes 12602368 | tf_op jit(solution)/shard_map/convert_element_type | solution.py:85
  86.5 5.4 %fusion.50 = f32[768,256]{1,0:T(8,128)S(1)} fusion(bf16[64,256]{1,0:T(8,128)(2,1)S(1)} %copy-done.9, bf16[768,4096]{1,0:T(8,128)(2,1)} %fusion.1, bf16[4096,64]{0,1:T(8,128)(2,1)S(1)} %copy-done, f32[256]{0:T(256)S(1)} %copy-done.10), kind=kOutput, calls=%fused_computation.51 | convolution fusion | flops 429834240 | bytes 7635968 | tf_op jit(solution)/shard_map/dot_general | solution.py:163
  93.1 8.4 %all-gather.2 = bf16[4,2,128]{2,1,0:T(2,128)(2,1)S(1)} all-gather(bf16[1,2,128]{2,1,0:T(2,128)(2,1)S(1)} %fusion.118), channel_id=2, replica_groups=mesh['sp_0'=4,'sp_1'=4,'tp'=8] {'sp_1'}, dimensions={0}, use_global_device_ids=true | all-gather | bytes 2560 | tf_op jit(solution)/shard_map/all_gather | solution.py:48
  101.5 10.5 %all_gather.26 = bf16[4,2,128]{2,1,0:T(2,128)(2,1)S(1)} all-gather(bf16[1,2,128]{2,1,0:T(2,128)(2,1)S(1)} %get-tuple-element.96), channel_id=1, replica_groups=mesh['sp_0'=4,'sp_1'=4,'tp'=8] {'sp_0'}, dimensions={0}, use_global_device_ids=true | all-gather | bytes 2560 | tf_op jit(solution)/shard_map/all_gather | solution.py:48
  112.1 5.2 %fusion.35 = f32[768,256]{1,0:T(8,128)S(1)} fusion(bf16[768,4096]{1,0:T(8,128)(2,1)} %fusion.1, bf16[4096,1024]{1,0:T(8,128)(2,1)} %all-gather.6.cloned.1.call-done), kind=kOutput, calls=%fused_computation.37 | convolution fusion | flops 1611202560 | bytes 9175040 | tf_op jit(solution)/shard_map/dot_general | solution.py:93
  117.7 5.2 %fusion.41 = f32[768,256]{1,0:T(8,128)S(1)} fusion(bf16[768,4096]{1,0:T(8,128)(2,1)} %fusion.1, bf16[4096,1024]{1,0:T(8,128)(2,1)} %all-gather.6.cloned.1.call-done), kind=kOutput, calls=%fused_computation.39 | convolution fusion | flops 1611005952 | bytes 9175040 | tf_op jit(solution)/shard_map/dot_general | solution.py:93
  124.2 7.4 %fusion.14 = bf16[768,512]{1,0:T(8,128)(2,1)S(1)} fusion(bf16[768,4096]{1,0:T(8,128)(2,1)} %fusion.1, bf16[4096,1024]{1,0:T(8,128)(2,1)} %all-gather.6.cloned.1.call-done), kind=kOutput, calls=%fused_computation.28 | convolution fusion | flops 3221618688 | bytes 11272192 | tf_op jit(solution)/shard_map/dot_general | solution.py:93
  131.8 3.9 %copy_multiply_fusion = (f32[12,64,2,128]{3,0,1,2:T(8,128)S(1)}, f32[12,64,2,128]{3,0,1,2:T(8,128)}, f32[12,64,2,128]{3,0,1,2:T(8,128)}, f32[12,64,2,128]{3,0,1,2:T(8,128)S(1)}) fusion(f32[12,64,2,128]{3,2,1,0:T(2,128)} %reshape.239, f32[12,64,2,128]{3,0,1,2:T(8,128)} %copy-done.4, f32[12,2,128]{2,0,1:T(8,128)S(1)} %get-tuple-element.140, ...), kind=kLoop, calls=%fused_computation.41 | loop fusion | flops 1179648 | bytes 5529600 | tf_op jit(solution)/shard_map/mul | solution.py:122
  135.7 3.2 %fusion.52 = f32[12,2,128,256]{3,2,1,0:T(8,128)} fusion(f32[12,64,2,128]{3,0,1,2:T(8,128)S(1)} %get-tuple-element.85, bf16[12,64,2,256]{3,2,1,0:T(2,128)(2,1)S(1)} %reshape.235), kind=kOutput, calls=%fused_computation.63 | convolution fusion | flops 603979776 | bytes 4718592 | tf_op jit(solution)/shard_map/njhd,njhv->nhdv/dot_general | solution.py:128
  138.8 22.1 %while.13 = (s32[]{:T(128)}, f32[2,128,256]{2,1,0:T(8,128)S(1)}, f32[12,2,128,256]{3,2,1,0:T(8,128)}, f32[12,2,128]{2,0,1:T(8,128)S(1)}, f32[12,2,128,256]{3,2,1,0:T(8,128)}, /*index=5*/s32[]{:T(128)}, s32[]{:T(128)}) while((s32[]{:T(128)}, f32[2,128,256]{2,1,0:T(8,128)S(1)}, f32[12,2,128,256]{3,2,1,0:T(8,128)}, ...), condition=%wide.region_3.4_spmd.clone, body=%wide.region_2.3_spmd.clone.sunk | while | flops 262147 | bytes 1316448 | solution.py:135
  161.0 13.7 %all-gather.1 = bf16[8,128,256]{2,1,0:T(8,128)(2,1)S(1)} all-gather(bf16[2,128,256]{2,1,0:T(8,128)(2,1)S(1)} %convert_element_type.304), channel_id=3, replica_groups=mesh['sp_0'=4,'sp_1'=4,'tp'=8] {'sp_1'}, dimensions={0}, use_global_device_ids=true | all-gather | bytes 655360 | tf_op jit(solution)/shard_map/all_gather | solution.py:48
  174.9 10.4 %all_gather.29 = bf16[4,2,128,256]{3,2,1,0:T(8,128)(2,1)S(1)} all-gather(bf16[1,2,128,256]{3,2,1,0:T(8,128)(2,1)S(1)} %fusion.78), channel_id=1, replica_groups=mesh['sp_0'=4,'sp_1'=4,'tp'=8] {'sp_0'}, dimensions={0}, use_global_device_ids=true | all-gather | bytes 655360 | tf_op jit(solution)/shard_map/all_gather | solution.py:48
  185.3 3.0 %convolution_select_fusion = f32[12,2,64,64]{3,2,1,0:T(8,128)S(1)} fusion(f32[12,64,2,128]{3,0,1,2:T(8,128)} %get-tuple-element.86, f32[12,64,2,128]{3,0,1,2:T(8,128)S(1)} %get-tuple-element.91, pred[64,64]{1,0:T(8,128)(4,1)S(1)} %iota_compare_fusion), kind=kOutput, calls=%fused_computation.32 | convolution fusion | flops 151093248 | bytes 1970176 | tf_op jit(solution)/shard_map/nihd,njhd->nhij/dot_general | solution.py:124
  191.3 3.4 %multiply_reduce_fusion.1 = (f32[12,64,2]{1,2,0:T(2,128)S(1)}, f32[12,64,2,256]{3,1,2,0:T(8,128)}) fusion(f32[12,64,2,128]{3,0,1,2:T(8,128)S(1)} %copy-done.6, bf16[4,2,128,256]{3,2,1,0:T(8,128)(2,1)S(1)} %all_gather.29, f32[2,128]{1,0:T(2,128)S(1)} %get-tuple-element.97, f32[2,128]{1,0:T(2,128)S(1)} %get-tuple-element.103, ...), kind=kOutput, calls=%fused_computation.27 | convolution fusion | flops 607648256 | bytes 6568968 | tf_op jit(solution)/shard_map/nihd,hdv->nihv/dot_general | solution.py:178
  198.8 7.4 %fusion.17 = bf16[768,512]{1,0:T(8,128)(2,1)S(1)} fusion(bf16[768,4096]{1,0:T(8,128)(2,1)} %fusion.1, bf16[4096,1536]{1,0:T(8,128)(2,1)} %all-gather.8.cloned.1.call-done), kind=kOutput, calls=%fused_computation.29 | convolution fusion | flops 3221618688 | bytes 11272192 | tf_op jit(solution)/shard_map/dot_general | solution.py:93
  206.3 7.6 %multiply_convert_fusion.1 = bf16[768,512]{1,0:T(8,128)(2,1)S(1)} fusion(bf16[768,512]{1,0:T(8,128)(2,1)S(1)} %fusion.17, bf16[768,4096]{1,0:T(8,128)(2,1)} %fusion.1, bf16[4096,1536]{1,0:T(8,128)(2,1)} %all-gather.8.cloned.1.call-done), kind=kOutput, calls=%fused_computation.25 | convolution fusion | flops 3223191552 | bytes 12058624 | tf_op jit(solution)/shard_map/dot_general | solution.py:93
  215.2 6.4 %fusion.48 = f32[768,4096]{1,0:T(8,128)} fusion(bf16[512,4096]{1,0:T(8,128)(2,1)S(1)} %copy-done.5, f32[768,512]{1,0:T(8,128)S(1)} %bitcast.205, f32[768,512]{1,0:T(8,128)S(1)} %bitcast.204, f32[512]{0:T(512)S(1)} %bitcast.210), kind=kOutput, calls=%fused_computation.49 | convolution fusion | flops 3222405120 | bytes 19924992 | tf_op jit(solution)/shard_map/dot_general | solution.py:254
  221.6 15.3 %add_convert_fusion = bf16[768,4096]{1,0:T(8,128)(2,1)} fusion(f32[768,4096]{1,0:T(8,128)} %fusion.48, bf16[512,4096]{1,0:T(8,128)(2,1)} %param.33, bf16[768,512]{1,0:T(8,128)(2,1)S(1)} %multiply_convert_fusion.1, bf16[768,4096]{1,0:T(8,128)(2,1)} %fusion.1, bf16[4096,1536]{1,0:T(8,128)(2,1)} %all-gather.8.cloned.1.call-done, ...), kind=kOutput, calls=%fused_computation.8 | convolution fusion | flops 6455820288 | bytes 34349056 | tf_op jit(solution)/shard_map/dot_general | solution.py:255
  236.9 51.6 %reduce-scatter.2.cloned.1.call-done = bf16[96,4096]{1,0:T(8,128)(2,1)} async-done(((bf16[768,4096]{1,0:T(8,128)(2,1)}), bf16[96,4096]{1,0:T(8,128)(2,1)}) %reduce-scatter.2.cloned.1.call-update) | async-done | bytes 786448 | tf_op jit(solution)/shard_map/reduce_scatter | solution.py:252
  (130 shorter events, 50.1 us)
Async XLA Ops:
  6.5 80.0 %copy-start = (bf16[4096,64]{0,1:T(8,128)(2,1)S(1)}, bf16[4096,64]{0,1:T(8,128)(2,1)}, u32[]{:S(2)}) copy-start(bf16[4096,64]{0,1:T(8,128)(2,1)} %param.26) | copy-start | bytes 1572868
  6.5 105.5 %all-gather.6.cloned.1.call-start = ((), (), s32[]{:S(2)}) async-start(), calls=%async_computation.1 | async-start | bytes 8912896 | tf_op jit(solution)/shard_map/all_gather | solution.py:71
  8.5 54.0 %copy-start.8 = (bf16[96,4096]{1,0:T(8,128)(2,1)S(1)}, bf16[96,4096]{1,0:T(8,128)(2,1)}, u32[]{:S(2)}) copy-start(bf16[96,4096]{1,0:T(8,128)(2,1)} %param.18) | copy-start | bytes 2359300
  8.5 190.3 %all-gather.8.cloned.1.call-start = ((), (), s32[]{:S(2)}) async-start(), calls=%async_computation.2 | async-start | bytes 13369344 | tf_op jit(solution)/shard_map/all_gather | solution.py:71
  8.6 11.9 %collective-permute-start = (bf16[96,4096]{1,0:T(8,128)(2,1)}, bf16[96,4096]{1,0:T(8,128)(2,1)S(1)}, u32[]{:S(2)}, u32[]{:S(2)}) collective-permute-start(bf16[96,4096]{1,0:T(8,128)(2,1)} %param.18), channel_id=1, source_target_pairs={{0,1},{1,2},{2,3},{3,4},{4,5},{5,6},{6,7},{7,0},{8,9},{9,10},{10,1... | collective-permute-start | bytes 2359304 | tf_op jit(solution)/shard_map/ppermute | solution.py:27
  20.4 11.3 %collective-permute-start.1 = (bf16[96,4096]{1,0:T(8,128)(2,1)S(1)}, bf16[96,4096]{1,0:T(8,128)(2,1)}, u32[]{:S(2)}, u32[]{:S(2)}) collective-permute-start(bf16[96,4096]{1,0:T(8,128)(2,1)S(1)} %collective-permute-done), channel_id=1, source_target_pairs={{0,1},{1,2},{2,3},{3,4},{4,5},{5,6},{6,7},{7,0},{8,9},{9,10},{10,1... | collective-permute-start | bytes 2359304 | tf_op jit(solution)/shard_map/ppermute | solution.py:27
  22.8 13.7 %collective-permute-start.4 = (bf16[96,4096]{1,0:T(8,128)(2,1)}, bf16[96,4096]{1,0:T(8,128)(2,1)S(1)}, u32[]{:S(2)}, u32[]{:S(2)}) collective-permute-start(bf16[96,4096]{1,0:T(8,128)(2,1)} %param.18), channel_id=1, source_target_pairs={{1,0},{2,1},{3,2},{4,3},{5,4},{6,5},{7,6},{0,7},{9,8},{10,9},{11,1... | collective-permute-start | bytes 2359304 | tf_op jit(solution)/shard_map/ppermute | solution.py:29
  31.7 11.8 %collective-permute-start.2 = (bf16[96,4096]{1,0:T(8,128)(2,1)}, bf16[96,4096]{1,0:T(8,128)(2,1)}, u32[]{:S(2)}, u32[]{:S(2)}) collective-permute-start(bf16[96,4096]{1,0:T(8,128)(2,1)} %collective-permute-done.1), channel_id=1, source_target_pairs={{0,1},{1,2},{2,3},{3,4},{4,5},{5,6},{6,7},{7,0},{8,9},{9,10},{10,1... | collective-permute-start | bytes 2359304 | tf_op jit(solution)/shard_map/ppermute | solution.py:27
  36.4 252.0 %reduce-scatter.2.cloned.1.call-start = ((), (), s32[]{:S(2)}) async-start(), calls=%async_computation.3 | async-start | bytes 7077888 | tf_op jit(solution)/shard_map/reduce_scatter | solution.py:252
  36.5 12.7 %collective-permute-start.5 = (bf16[96,4096]{1,0:T(8,128)(2,1)S(1)}, bf16[96,4096]{1,0:T(8,128)(2,1)}, u32[]{:S(2)}, u32[]{:S(2)}) collective-permute-start(bf16[96,4096]{1,0:T(8,128)(2,1)S(1)} %collective-permute-done.4), channel_id=1, source_target_pairs={{1,0},{2,1},{3,2},{4,3},{5,4},{6,5},{7,6},{0,7},{9,8},{10,9},{11,1... | collective-permute-start | bytes 2359304 | tf_op jit(solution)/shard_map/ppermute | solution.py:29
  43.6 11.7 %collective-permute-start.3 = (bf16[96,4096]{1,0:T(8,128)(2,1)}, bf16[96,4096]{1,0:T(8,128)(2,1)}, u32[]{:S(2)}, u32[]{:S(2)}) collective-permute-start(bf16[96,4096]{1,0:T(8,128)(2,1)} %collective-permute-done.2), channel_id=1, source_target_pairs={{0,1},{1,2},{2,3},{3,4},{4,5},{5,6},{6,7},{7,0},{8,9},{9,10},{10,1... | collective-permute-start | bytes 2359304 | tf_op jit(solution)/shard_map/ppermute | solution.py:27
  49.2 17.4 %collective-permute-start.6 = (bf16[96,4096]{1,0:T(8,128)(2,1)}, bf16[96,4096]{1,0:T(8,128)(2,1)S(1)}, u32[]{:S(2)}, u32[]{:S(2)}) collective-permute-start(bf16[96,4096]{1,0:T(8,128)(2,1)} %collective-permute-done.5), channel_id=1, source_target_pairs={{1,0},{2,1},{3,2},{4,3},{5,4},{6,5},{7,6},{0,7},{9,8},{10,9},{11,1... | collective-permute-start | bytes 2359304 | tf_op jit(solution)/shard_map/ppermute | solution.py:29
  78.3 8.2 %copy-start.9 = (bf16[64,256]{1,0:T(8,128)(2,1)S(1)}, bf16[64,256]{1,0:T(8,128)(2,1)}, u32[]{:S(2)}) copy-start(bf16[64,256]{1,0:T(8,128)(2,1)} %param.27) | copy-start | bytes 98308
  78.3 8.2 %copy-start.10 = (f32[256]{0:T(256)S(1)}, f32[256]{0:T(256)}, u32[]{:S(2)}) copy-start(f32[256]{0:T(256)} %param.28) | copy-start | bytes 3076
  93.0 24.2 %copy-start.4 = (f32[12,64,2,128]{3,0,1,2:T(8,128)}, f32[12,64,2,128]{3,0,1,2:T(8,128)S(1)}, u32[]{:S(2)}) copy-start(f32[12,64,2,128]{3,0,1,2:T(8,128)S(1)} %fusion.46) | copy-start | bytes 2359300
  161.0 28.2 %copy-start.7 = (f32[12,2,128,256]{3,2,1,0:T(8,128)S(1)}, f32[12,2,128,256]{3,2,1,0:T(8,128)}, u32[]{:S(2)}) copy-start(f32[12,2,128,256]{3,2,1,0:T(8,128)} %get-tuple-element.33) | copy-start | bytes 9437188
  188.4 2.9 copy-start.6
  194.9 1.4 copy-start.3
  206.2 8.9 %copy-start.2 = (f32[96,8,2,256]{3,1,2,0:T(8,128)S(1)}, f32[96,8,2,256]{3,1,2,0:T(8,128)}, u32[]{:S(2)}) copy-start(f32[96,8,2,256]{3,1,2,0:T(8,128)} %copy.75) | copy-start | bytes 4718596
  206.3 8.9 %copy-start.5 = (bf16[512,4096]{1,0:T(8,128)(2,1)S(1)}, bf16[512,4096]{1,0:T(8,128)(2,1)}, u32[]{:S(2)}) copy-start(bf16[512,4096]{1,0:T(8,128)(2,1)} %param.32) | copy-start | bytes 12582916
  213.8 7.7 %collective-permute-start.7 = (bf16[2,512]{1,0:T(2,128)(2,1)S(1)}, bf16[2,512]{1,0:T(2,128)(2,1)S(1)}, u32[]{:S(2)}, u32[]{:S(2)}) collective-permute-start(bf16[2,512]{1,0:T(2,128)(2,1)S(1)} %slice.153), channel_id=1, source_target_pairs={{0,8},{8,16},{16,24},{24,32},{32,40},{40,48},{48,56},{56,64},{64,7... | collective-permute-start | bytes 6152 | tf_op jit(solution)/shard_map/ppermute | solution.py:66
  221.6 66.9 %copy-start.1 = (bf16[4096,64]{0,1:T(8,128)(2,1)S(1)}, bf16[4096,64]{0,1:T(8,128)(2,1)}, u32[]{:S(2)}) copy-start(bf16[4096,64]{0,1:T(8,128)(2,1)} %param.26) | copy-start | bytes 1572868
Sparse Core Ops, SparseCore 0:
  9.5 73.9 all-gather.5
  85.6 91.4 all-gather.7
  237.0 51.3 reduce-scatter.1
